TPU v7x, 512 devices: a whole 4x8x8 slice. The times are simulated.
512 devices in a mesh: ep: 32 (over z, x), tp: 16 (over y, core).
Axes of the slice: x: 4, y: 8, z: 8, core: 2. Of those that a mesh axis runs over, the one named last changes fastest.
Arguments:
- residual: bfloat16 [256, 2048], P(None, 'ep'), may hold values from -40 to 40
- norm_gain: float32 [2048], P('ep'), may hold values from 0.1 to 1.9
- query_weight: bfloat16 [2048, 2048], P('ep', 'tp'), may hold values from -0.125 to 0.125
- key_weight: bfloat16 [2048, 2048], P('ep', 'tp'), may hold values from -0.125 to 0.125
- value_weight: bfloat16 [2048, 4096], P('ep', 'tp'), may hold values from -0.125 to 0.125
- gate_weight: bfloat16 [2048, 4096], P('ep', 'tp'), may hold values from -0.125 to 0.125
- out_weight: bfloat16 [4096, 2048], P('tp', 'ep'), may hold values from -0.09375 to 0.09375
- prior_state: float32 [256, 16, 128, 256], P('ep', 'tp'), may hold values from -3 to 3
- lengths: int32 [256], P('ep'), may hold values from 1024 to 16383
- ffn_gain: float32 [2048], replicated, may hold values from 0.1 to 1.9
- expert_gate: bfloat16 [32, 2048, 2048], P('ep', None, 'tp'), may hold values from -0.5 to 0.5
- expert_up: bfloat16 [32, 2048, 2048], P('ep', None, 'tp'), may hold values from -0.5 to 0.5
- expert_down: bfloat16 [32, 2048, 2048], P('ep', 'tp'), may hold values from -0.03125 to 0.03125
- route_ids: int32 [256, 4], replicated, may hold values from 0 to 31, all different within a row; in each aligned block of 8 rows (0 to 7, 8 to 15, ...) at most 2 rows name the same one
- route_weight: float32 [256, 4], replicated, may hold values from 0.1 to 1
- dense_gate: bfloat16 [2048, 2048], P('ep', 'tp'), may hold values from -0.125 to 0.125
- dense_up: bfloat16 [2048, 2048], P('ep', 'tp'), may hold values from -0.125 to 0.125
- dense_down: bfloat16 [2048, 2048], P('tp', 'ep'), may hold values from -0.25 to 0.25
- mix_vector: bfloat16 [2048], P('ep'), may hold values from -0.125 to 0.125
Outputs:
- layer_out: bfloat16 [256, 2048], P(None, 'ep')
- new_state: float32 [256, 16, 128, 256], P('ep', 'tp')
Inputs may be any that keep to these rules, and one draw needn't show every extreme that they name: `route_ids`: each row names 4 different experts; within each aligned block of 8 rows no expert is named by more than 2 rows, and in some block one expert is named by exactly 2 rows.
All inputs are finite; a program needn't handle non-finite values.
Results may differ from a plain program's by a relative error of at most 0.02.
Values may be sent and summed in bfloat16 or wider, within the bound.
No kernel may reach another device: no remote copies, remote signals or barrier semaphores. Data moves between devices by JAX's collectives and lax.ppermute only.
A program may use at most 64 MiB of HBM per device.

v0:
```python
import math
import jax
import jax.numpy as jnp
from jax import lax
from jax.sharding import PartitionSpec as P

D = 2048
KEY_DIM = 128
VAL_DIM = 256
norm_eps = 1e-06
clamp_limit = 7.0
gate_alpha = 1.702


def split_up(value, dim, peers):
    shape = value.shape
    pieces = value.reshape(*shape[:dim], peers, shape[dim] // peers, *shape[dim + 1 :])
    return jnp.moveaxis(pieces, dim, 0)


def summed_on_arrival(value, axis, dim):
    pieces = split_up(value, dim, lax.axis_size(axis))
    arrived = lax.all_to_all(pieces, axis, split_axis=0, concat_axis=0, tiled=True)
    return arrived.sum(axis=0)


def in_one_piece(arrays, axis, dim, along):
    widths = [math.prod(a.shape[along:]) for a in arrays]
    both = jnp.concatenate(
        [a.reshape(*a.shape[:along], w) for a, w in zip(arrays, widths)], axis=along
    )
    filled = summed_on_arrival(both, axis, dim)
    pieces = jnp.split(filled, [sum(widths[:k]) for k in range(1, len(widths))], axis=along)
    return tuple(
        (b.reshape(*filled.shape[:along], *a.shape[along:]) for a, b in zip(arrays, pieces))
    )


def from_everyone(value, axis):
    peers = lax.axis_size(axis)
    return lax.all_to_all(
        jnp.broadcast_to(value[None], (peers, *value.shape)), axis, 0, 0, tiled=True
    )


def laid_out(pieces, dim):
    shape = list(pieces.shape[1:])
    shape[dim] *= pieces.shape[0]
    return jnp.moveaxis(pieces, 0, dim).reshape(shape)


def gather_directly(value, axis, dim):
    pieces = from_everyone(value, axis)
    return laid_out(pieces, dim)


def total_of_pieces(value, axis):
    pieces = lax.all_gather(value, axis).astype(jnp.float32)
    return pieces.sum(axis=0)


def sum_at_owner(value, axis, dim):
    pieces = split_up(value, dim, lax.axis_size(axis))
    arrived = lax.all_to_all(pieces, axis, split_axis=0, concat_axis=0, tiled=True)
    return arrived.astype(jnp.float32).sum(axis=0)


def padded_to(lines, peers):
    spare = -lines.shape[0] % peers
    if not spare:
        return lines
    return jnp.concatenate([lines, jnp.zeros((spare, *lines.shape[1:]), lines.dtype)])


def nested_sum(value, axes):
    lines = value.reshape(-1, value.shape[-1])
    own = sum_at_owner(padded_to(lines, lax.axis_size(axes)), axes, 0)
    whole = gather_directly(own.astype(jnp.bfloat16), axes, 0)
    return whole[: len(lines)].reshape(value.shape).astype(jnp.float32)


def sum_by_parts(value, axes):
    padded = padded_to(value, lax.axis_size(axes))
    whole = gather_directly(summed_on_arrival(padded, axes, 0), axes, 0)
    return lax.slice_in_dim(whole, 0, len(value)).reshape(value.shape)


def in_one(arrays, axis):
    ends = [0]
    for a in arrays:
        ends.append(ends[-1] + a.size)
    subtotal = sum_by_parts(jnp.concatenate([a.ravel() for a in arrays]), axis)
    return tuple((subtotal[b:e].reshape(a.shape) for a, b, e in zip(arrays, ends, ends[1:])))


def rotate_half(vectors, positions):
    half_dim = vectors.shape[-1] // 2
    inverse = 1.0 / 10000.0 ** jnp.linspace(0.0, 1.0, half_dim, dtype=jnp.float32)
    angles = positions.astype(jnp.float32)[:, None] * inverse[None, :]
    cosine = jnp.cos(angles)[:, None, :]
    sine_part = jnp.sin(angles)[:, None, :]
    first_half = vectors[..., :half_dim]
    second_half = vectors[..., half_dim:]
    return jnp.concatenate(
        [
            first_half * cosine - second_half * sine_part,
            second_half * cosine + first_half * sine_part,
        ],
        axis=-1,
    )


def slot_index(route_ids, groups, capacity, experts):
    pair_ids = route_ids.reshape(groups, -1)
    labels = jnp.arange(experts, dtype=jnp.int32)
    onehot = (pair_ids[:, :, None] == labels[None, None, :]).astype(jnp.int32)
    earlier = jnp.cumsum(onehot, axis=1) - onehot
    within = jnp.sum(earlier * onehot, axis=2)
    offset = jnp.arange(groups, dtype=jnp.int32)[:, None] * capacity
    return (pair_ids * (groups * capacity) + offset + within).reshape(-1)


def source_rows(target, total_rows, topk_count, table_size):
    owners = jnp.arange(target.shape[0], dtype=jnp.int32) // topk_count
    return jnp.full((table_size,), total_rows, jnp.int32).at[target].set(owners)


def rounded_product(left_rows, right_rows):
    partial_value = jnp.dot(left_rows, right_rows, preferred_element_type=jnp.float32)
    return lax.optimization_barrier(partial_value.astype(jnp.bfloat16))


def per_device(
    residual,
    norm_gain,
    query_weight,
    key_weight,
    value_weight,
    gate_weight,
    out_weight,
    prior_state,
    lengths,
    ffn_gain,
    expert_gate,
    expert_up,
    expert_down,
    route_ids,
    route_weight,
    dense_gate,
    dense_up,
    dense_down,
    mix_vector,
):
    ep_count = lax.axis_size("ep")
    ep_index = lax.axis_index("ep")
    batch_rows, local_width = residual.shape
    own_rows = batch_rows // ep_count
    topk_count = route_ids.shape[1]
    residual_float = residual.astype(jnp.float32)
    squares = jnp.sum(residual_float * residual_float, axis=1)
    normed_in = (residual_float * norm_gain).astype(jnp.bfloat16)
    all_weights = jnp.concatenate([query_weight, key_weight, value_weight, gate_weight], axis=1)
    whole_terms = jnp.dot(normed_in, all_weights, preferred_element_type=jnp.float32)
    projected, own_squares = in_one_piece((whole_terms, squares), "ep", 0, 1)
    row_scale = lax.rsqrt(own_squares / D + norm_eps)[:, None]
    key_cols = query_weight.shape[1]
    value_cols = value_weight.shape[1]
    heads_here = key_cols // KEY_DIM
    projected = projected * row_scale
    query_rot = rotate_half(projected[:, :key_cols].reshape(own_rows, heads_here, KEY_DIM), lengths)
    key_rot = rotate_half(
        projected[:, key_cols : 2 * key_cols].reshape(own_rows, heads_here, KEY_DIM), lengths
    ) * KEY_DIM ** (-0.5)
    values = projected[:, 2 * key_cols : 2 * key_cols + value_cols].reshape(
        own_rows, heads_here, VAL_DIM
    )
    gate_pre = projected[:, 2 * key_cols + value_cols :].reshape(own_rows, heads_here, VAL_DIM)
    head_ids = lax.axis_index("tp") * heads_here + jnp.arange(heads_here, dtype=jnp.int32)
    decay_rate = 1.0 - jnp.exp2(-1.0 - 0.5 * head_ids.astype(jnp.float32))
    new_state = (
        decay_rate[None, :, None, None] * prior_state
        + key_rot[:, :, :, None] * values[:, :, None, :]
    )
    state_read = jnp.einsum("bhk,bhkv->bhv", query_rot, new_state, precision=lax.Precision.HIGHEST)
    normed = state_read * lax.rsqrt(
        jnp.mean(state_read * state_read, axis=-1, keepdims=True) + norm_eps
    )
    gated_out = (
        (normed * jax.nn.silu(gate_pre))
        .astype(jnp.bfloat16)
        .reshape(own_rows, heads_here * VAL_DIM)
    )
    head_terms = rounded_product(gather_directly(gated_out, "ep", 0), out_weight)
    attn_out = total_of_pieces(head_terms.astype(jnp.float32).astype(jnp.bfloat16), "tp").astype(
        jnp.float32
    )
    after_mixer = (residual_float + attn_out).astype(jnp.bfloat16)
    capacity = max(2, 2 * own_rows * topk_count // ep_count)
    slot_count = ep_count * capacity
    target = slot_index(route_ids, ep_count, capacity, ep_count)
    slot_source = source_rows(target, batch_rows, topk_count, ep_count * slot_count)
    padded = jnp.concatenate([after_mixer, jnp.zeros((1, local_width), jnp.bfloat16)], axis=0)
    outgoing = padded[slot_source].reshape(ep_count, slot_count, local_width)
    arrived = lax.all_to_all(outgoing, "ep", split_axis=0, concat_axis=2, tiled=True)[0]
    rows_float = arrived.astype(jnp.float32)
    row_norm = lax.rsqrt(jnp.mean(rows_float * rows_float, axis=1, keepdims=True) + norm_eps)
    normed_rows = (rows_float * ffn_gain).astype(jnp.bfloat16)
    gate_val = jnp.minimum(
        jnp.dot(normed_rows, expert_gate[0], preferred_element_type=jnp.float32) * row_norm,
        clamp_limit,
    )
    up_val = jnp.clip(
        jnp.dot(normed_rows, expert_up[0], preferred_element_type=jnp.float32) * row_norm,
        -clamp_limit,
        clamp_limit,
    )
    hidden = ((up_val + 1.0) * gate_val * jax.nn.sigmoid(gate_alpha * gate_val)).astype(
        jnp.bfloat16
    )
    expert_part = rounded_product(hidden, expert_down[0]).astype(jnp.float32)
    expert_sum = nested_sum(expert_part.astype(jnp.bfloat16), "tp").astype(jnp.bfloat16)
    returned = lax.all_to_all(expert_sum[None], "ep", split_axis=2, concat_axis=0, tiled=True)
    picked = returned.reshape(ep_count * slot_count, local_width)[target]
    picked = picked.reshape(batch_rows, topk_count, local_width).astype(jnp.float32)
    routed = jnp.sum(picked * route_weight[:, :, None], axis=1)
    after_float = after_mixer.astype(jnp.float32)
    gain_here = lax.dynamic_slice_in_dim(ffn_gain, ep_index * local_width, local_width, 0)
    normed_ffn = (after_float * gain_here).astype(jnp.bfloat16)
    dense_cols = dense_gate.shape[1]
    both_terms = jnp.dot(
        normed_ffn,
        jnp.concatenate([dense_gate, dense_up], axis=1),
        preferred_element_type=jnp.float32,
    )
    mix_term = jnp.dot(normed_ffn, mix_vector, preferred_element_type=jnp.float32)
    both_terms, ffn_squares, mix_logit = in_one(
        (both_terms, jnp.sum(after_float * after_float, axis=1), mix_term), "ep"
    )
    ffn_scale = lax.rsqrt(ffn_squares / D + norm_eps)[:, None]
    dense_act = (
        jax.nn.silu(both_terms[:, :dense_cols] * ffn_scale)
        * (both_terms[:, dense_cols:] * ffn_scale)
    ).astype(jnp.bfloat16)
    dense_part = rounded_product(dense_act, dense_down).astype(jnp.float32)
    dense_out = total_of_pieces(dense_part.astype(jnp.bfloat16), "tp").astype(jnp.float32)
    dense_mix = jax.nn.sigmoid(ffn_scale[:, 0] * mix_logit)
    layer_out = (after_float + routed + dense_mix[:, None] * dense_out).astype(jnp.bfloat16)
    return (layer_out, new_state)


def solution(mesh):
    placed = (
        P(None, "ep"),
        P("ep"),
        P("ep", "tp"),
        P("ep", "tp"),
        P("ep", "tp"),
        P("ep", "tp"),
        P("tp", "ep"),
        P("ep", "tp", None, None),
        P("ep"),
        P(),
        P("ep", None, "tp"),
        P("ep", None, "tp"),
        P("ep", "tp", None),
        P(),
        P(),
        P("ep", "tp"),
        P("ep", "tp"),
        P("tp", "ep"),
        P("ep"),
    )
    return jax.shard_map(
        per_device,
        mesh=mesh,
        in_specs=placed,
        out_specs=(P(None, "ep"), P("ep", "tp", None, None)),
        check_vma=False,
    )
```

profile of v0, /device:TPU:1, one launch (start us, length us, event | category | flops | bytes accessed | tf_op | source)
XLA Modules:
  0.0 217.2 jit_solution(9277276090891454630)
XLA Ops:
  3.7 13.8 %all-to-all-start = ((f32[32,8,769]{2,1,0:T(8,128)}), f32[32,8,769]{2,1,0:T(8,128)S(1)}, u32[]{:S(2)}, u32[]{:S(2)}) async-start(f32[32,8,769]{2,1,0:T(8,128)} %pad_maximum_fusion), calls=%async_computation | async-start | bytes 1835008 | tf_op jit(solution)/shard_map/all_to_all | solution.py:23
  19.7 21.4 %all-to-all-done = f32[32,8,769]{2,1,0:T(8,128)S(1)} async-done(((f32[32,8,769]{2,1,0:T(8,128)}), f32[32,8,769]{2,1,0:T(8,128)S(1)}, u32[]{:S(2)}, u32[]{:S(2)}) %all-to-all-start) | async-done | bytes 787488 | tf_op jit(solution)/shard_map/all_to_all | solution.py:23
  43.4 6.0 %all-to-all-start.1 = ((bf16[32,8,256]{2,1,0:T(8,128)(2,1)}), bf16[32,8,256]{2,1,0:T(8,128)(2,1)S(1)}, u32[]{:S(2)}, u32[]{:S(2)}) async-start(bf16[32,8,256]{2,1,0:T(8,128)(2,1)} %broadcast_in_dim.13), calls=%async_computation.1 | async-start | bytes 262144 | tf_op jit(solution)/shard_map/all_to_all | solution.py:41
  50.3 4.3 %scatter_custom_fusion = s32[2048]{0:T(1024)S(1)} fusion(s32[1024]{0:T(1024)S(1)} %bitcast.88, s32[1024]{0:T(1024)S(1)} %add_select_fusion, s32[]{:T(128)} %constant.47.clone.1), kind=kCustom, calls=%fused_computation.117 | custom fusion | bytes 8196 | tf_op jit(solution)/shard_map/scatter | solution.py:125
  54.6 4.3 %all-to-all-done.1 = bf16[32,8,256]{2,1,0:T(8,128)(2,1)S(1)} async-done(((bf16[32,8,256]{2,1,0:T(8,128)(2,1)}), bf16[32,8,256]{2,1,0:T(8,128)(2,1)S(1)}, u32[]{:S(2)}, u32[]{:S(2)}) %all-to-all-start.1) | async-done | bytes 131104 | tf_op jit(solution)/shard_map/all_to_all | solution.py:41
  59.0 22.2 %all-gather = bf16[4096,64]{0,1:T(8,128)(2,1)S(1)} all-gather(bf16[256,64]{0,1:T(8,128)(2,1)S(1)} %convolution_convert_fusion.2), channel_id=2, replica_groups=mesh['ep'=32,'tp'=16] {'tp'}, dimensions={0}, use_global_device_ids=true | all-gather | bytes 557056 | tf_op jit(solution)/shard_map/all_gather | solution.py:58
  83.7 6.2 %gather_fusion = bf16[2048,64]{1,0:T(8,128)(2,1)S(1)} fusion(bf16[257,64]{1,0:T(8,128)(2,1)S(1)} %concatenate.47, s32[2048]{0:T(1024)S(1)} %fusion.55), kind=kCustom, calls=%fused_computation | custom fusion | bytes 532480 | tf_op jit(solution)/shard_map/gather | solution.py:203
  89.8 1.1 reshape.350
  90.9 4.1 %all-to-all-start.2 = ((bf16[32,2,2048]{2,1,0:T(2,128)(2,1)}), bf16[32,2,2048]{2,1,0:T(2,128)(2,1)S(1)}, u32[]{:S(2)}, u32[]{:S(2)}) async-start(bf16[32,2,2048]{2,1,0:T(2,128)(2,1)} %reshape.350), calls=%async_computation.2 | async-start | bytes 524288 | tf_op jit(solution)/shard_map/all_to_all | solution.py:204
  95.0 1.1 all_to_all.48
  96.1 10.5 %all-to-all-done.2 = bf16[32,2,2048]{2,1,0:T(2,128)(2,1)S(1)} async-done(((bf16[32,2,2048]{2,1,0:T(2,128)(2,1)}), bf16[32,2,2048]{2,1,0:T(2,128)(2,1)S(1)}, u32[]{:S(2)}, u32[]{:S(2)}) %all-to-all-start.2) | async-done | bytes 262176 | tf_op jit(solution)/shard_map/all_to_all | solution.py:204
  106.6 4.5 %all-to-all-start.6 = ((f32[32,1,2064]{2,1,0:T(1,128)}), f32[32,1,2064]{2,1,0:T(1,128)S(1)}, u32[]{:S(2)}, u32[]{:S(2)}) async-start(f32[32,1,2064]{2,1,0:T(1,128)} %all_to_all.48), calls=%async_computation.6 | async-start | bytes 557056 | tf_op jit(solution)/shard_map/all_to_all | solution.py:23
  115.5 6.4 %all-to-all-done.6 = f32[32,1,2064]{2,1,0:T(1,128)S(1)} async-done(((f32[32,1,2064]{2,1,0:T(1,128)}), f32[32,1,2064]{2,1,0:T(1,128)S(1)}, u32[]{:S(2)}, u32[]{:S(2)}) %all-to-all-start.6) | async-done | bytes 264224 | tf_op jit(solution)/shard_map/all_to_all | solution.py:23
  121.9 7.8 %all-to-all-start.3 = ((bf16[16,4,2048]{2,1,0:T(4,128)(2,1)}), bf16[16,4,2048]{2,1,0:T(4,128)(2,1)S(1)}, u32[]{:S(2)}, u32[]{:S(2)}) async-start(bf16[16,4,2048]{2,1,0:T(4,128)(2,1)} %reshape.301), calls=%async_computation.3 | async-start | bytes 524288 | tf_op jit(solution)/shard_map/all_to_all | solution.py:64
  129.9 11.4 %all-to-all-done.3 = bf16[16,4,2048]{2,1,0:T(4,128)(2,1)S(1)} async-done(((bf16[16,4,2048]{2,1,0:T(4,128)(2,1)}), bf16[16,4,2048]{2,1,0:T(4,128)(2,1)S(1)}, u32[]{:S(2)}, u32[]{:S(2)}) %all-to-all-start.3) | async-done | bytes 262176 | tf_op jit(solution)/shard_map/all_to_all | solution.py:64
  142.1 3.9 %all-to-all-start.7 = ((f32[32,1,2064]{2,1,0:T(1,128)}), f32[32,1,2064]{2,1,0:T(1,128)S(1)}, u32[]{:S(2)}, u32[]{:S(2)}) async-start(f32[32,1,2064]{2,1,0:T(1,128)} %broadcast_in_dim.18), calls=%async_computation.7 | async-start | bytes 557056 | tf_op jit(solution)/shard_map/all_to_all | solution.py:41
  146.1 13.0 %all-to-all-done.7 = f32[32,1,2064]{2,1,0:T(1,128)S(1)} async-done(((f32[32,1,2064]{2,1,0:T(1,128)}), f32[32,1,2064]{2,1,0:T(1,128)S(1)}, u32[]{:S(2)}, u32[]{:S(2)}) %all-to-all-start.7) | async-done | bytes 264224 | tf_op jit(solution)/shard_map/all_to_all | solution.py:41
  159.9 3.9 %all-to-all-start.4 = ((bf16[16,4,2048]{2,1,0:T(4,128)(2,1)}), bf16[16,4,2048]{2,1,0:T(4,128)(2,1)S(1)}, u32[]{:S(2)}, u32[]{:S(2)}) async-start(bf16[16,4,2048]{2,1,0:T(4,128)(2,1)} %broadcast_in_dim.16), calls=%async_computation.4 | async-start | bytes 524288 | tf_op jit(solution)/shard_map/all_to_all | solution.py:41
  165.1 10.5 %all-to-all-done.4 = bf16[16,4,2048]{2,1,0:T(4,128)(2,1)S(1)} async-done(((bf16[16,4,2048]{2,1,0:T(4,128)(2,1)}), bf16[16,4,2048]{2,1,0:T(4,128)(2,1)S(1)}, u32[]{:S(2)}, u32[]{:S(2)}) %all-to-all-start.4) | async-done | bytes 262176 | tf_op jit(solution)/shard_map/all_to_all | solution.py:41
  176.9 11.5 %reduce.10 = bf16[2048,64]{1,0:T(8,128)(2,1)S(1)} reduce(bf16[2048,1,64]{2,1,0:T(2,128)(2,1)S(1)} %bitcast.80, bf16[]{:T(256)} %broadcast.245), dimensions={1}, to_apply=%bitcast.71.reduce_sub_computation | reduce | bytes 524290
  188.5 1.1 reshape.352
  189.6 4.4 %all-to-all-start.5 = ((bf16[32,2,2048]{2,1,0:T(2,128)(2,1)}), bf16[32,2,2048]{2,1,0:T(2,128)(2,1)S(1)}, u32[]{:S(2)}, u32[]{:S(2)}) async-start(bf16[32,2,2048]{2,1,0:T(2,128)(2,1)} %reshape.352), calls=%async_computation.5 | async-start | bytes 524288 | tf_op jit(solution)/shard_map/all_to_all | solution.py:222
  194.2 15.9 %all-gather.1 = bf16[4096,64]{0,1:T(8,128)(2,1)S(1)} all-gather(bf16[256,64]{0,1:T(8,128)(2,1)S(1)} %convolution_convert_fusion.1), channel_id=3, replica_groups=mesh['ep'=32,'tp'=16] {'tp'}, dimensions={0}, use_global_device_ids=true | all-gather | bytes 557056 | tf_op jit(solution)/shard_map/all_gather | solution.py:58
  212.8 3.2 %gather_fusion.1 = bf16[1024,64]{1,0:T(8,128)(2,1)S(1)} fusion(bf16[2048,64]{1,0:T(8,128)(2,1)S(1)} %bitcast.78, s32[1024]{0:T(1024)S(1)} %broadcast_clamp_fusion), kind=kCustom, calls=%fused_computation.1 | custom fusion | bytes 266240 | tf_op jit(solution)/shard_map/gather | solution.py:223
  (122 shorter events, 23.5 us)
Async XLA Ops:
  0.6 112.9 %copy-start = (bf16[1,128,2048]{2,1,0:T(8,128)(2,1)S(1)}, bf16[1,128,2048]{2,1,0:T(8,128)(2,1)}, u32[]{:S(2)}) copy-start(bf16[1,128,2048]{2,1,0:T(8,128)(2,1)} %param.33) | copy-start | bytes 1572868
  1.7 0.8 copy-start.5
  1.7 0.8 copy-start.6
  1.7 0.8 copy-start.8
  1.7 0.7 copy-start.9
  1.7 0.7 copy-start.15
  3.7 13.9 %copy-start.17 = (s32[8]{0:T(128)S(1)}, s32[8]{0:T(128)}, u32[]{:S(2)}) copy-start(s32[8]{0:T(128)} %param.29) | copy-start | bytes 100
  3.7 13.9 %copy-start.12 = (s32[256,4]{0,1:T(4,128)S(1)}, s32[256,4]{0,1:T(4,128)}, u32[]{:S(2)}) copy-start(s32[256,4]{0,1:T(4,128)} %param.34) | copy-start | bytes 12292
  3.7 37.4 %all-to-all-start = ((f32[32,8,769]{2,1,0:T(8,128)}), f32[32,8,769]{2,1,0:T(8,128)S(1)}, u32[]{:S(2)}, u32[]{:S(2)}) async-start(f32[32,8,769]{2,1,0:T(8,128)} %pad_maximum_fusion), calls=%async_computation | async-start | bytes 1835008 | tf_op jit(solution)/shard_map/all_to_all | solution.py:23
  17.6 24.1 %copy-start.2 = (f32[8,1,128,256]{3,2,1,0:T(8,128)S(1)}, f32[8,1,128,256]{3,2,1,0:T(8,128)}, u32[]{:S(2)}) copy-start(f32[8,1,128,256]{3,2,1,0:T(8,128)} %param.28) | copy-start | bytes 3145732
  41.9 39.3 %copy-start.1 = (f32[8,1,128,256]{3,2,1,0:T(8,128)}, f32[8,1,128,256]{3,2,1,0:T(8,128)S(1)}, u32[]{:S(2)}) copy-start(f32[8,1,128,256]{3,2,1,0:T(8,128)S(1)} %multiply_add_fusion) | copy-start | bytes 3145732
  43.4 15.4 %all-to-all-start.1 = ((bf16[32,8,256]{2,1,0:T(8,128)(2,1)}), bf16[32,8,256]{2,1,0:T(8,128)(2,1)S(1)}, u32[]{:S(2)}, u32[]{:S(2)}) async-start(bf16[32,8,256]{2,1,0:T(8,128)(2,1)} %broadcast_in_dim.13), calls=%async_computation.1 | async-start | bytes 262144 | tf_op jit(solution)/shard_map/all_to_all | solution.py:41
  49.4 9.4 %copy-start.7 = (bf16[256,64]{0,1:T(8,128)(2,1)S(1)}, bf16[256,64]{0,1:T(8,128)(2,1)}, u32[]{:S(2)}) copy-start(bf16[256,64]{0,1:T(8,128)(2,1)} %param.27) | copy-start | bytes 98308
  81.9 0.7 copy-start.11
  90.9 15.7 %all-to-all-start.2 = ((bf16[32,2,2048]{2,1,0:T(2,128)(2,1)}), bf16[32,2,2048]{2,1,0:T(2,128)(2,1)S(1)}, u32[]{:S(2)}, u32[]{:S(2)}) async-start(bf16[32,2,2048]{2,1,0:T(2,128)(2,1)} %reshape.350), calls=%async_computation.2 | async-start | bytes 524288 | tf_op jit(solution)/shard_map/all_to_all | solution.py:204
  106.6 15.3 %all-to-all-start.6 = ((f32[32,1,2064]{2,1,0:T(1,128)}), f32[32,1,2064]{2,1,0:T(1,128)S(1)}, u32[]{:S(2)}, u32[]{:S(2)}) async-start(f32[32,1,2064]{2,1,0:T(1,128)} %all_to_all.48), calls=%async_computation.6 | async-start | bytes 557056 | tf_op jit(solution)/shard_map/all_to_all | solution.py:23
  112.2 1.0 copy-start.3
  113.3 1.0 copy-start.4
  121.9 19.4 %all-to-all-start.3 = ((bf16[16,4,2048]{2,1,0:T(4,128)(2,1)}), bf16[16,4,2048]{2,1,0:T(4,128)(2,1)S(1)}, u32[]{:S(2)}, u32[]{:S(2)}) async-start(bf16[16,4,2048]{2,1,0:T(4,128)(2,1)} %reshape.301), calls=%async_computation.3 | async-start | bytes 524288 | tf_op jit(solution)/shard_map/all_to_all | solution.py:64
  142.1 17.0 %all-to-all-start.7 = ((f32[32,1,2064]{2,1,0:T(1,128)}), f32[32,1,2064]{2,1,0:T(1,128)S(1)}, u32[]{:S(2)}, u32[]{:S(2)}) async-start(f32[32,1,2064]{2,1,0:T(1,128)} %broadcast_in_dim.18), calls=%async_computation.7 | async-start | bytes 557056 | tf_op jit(solution)/shard_map/all_to_all | solution.py:41
  159.9 3.9 %copy-start.14 = (f32[256,4]{0,1:T(4,128)S(1)}, f32[256,4]{0,1:T(4,128)}, u32[]{:S(2)}) copy-start(f32[256,4]{0,1:T(4,128)} %param.35) | copy-start | bytes 12292
  159.9 15.7 %all-to-all-start.4 = ((bf16[16,4,2048]{2,1,0:T(4,128)(2,1)}), bf16[16,4,2048]{2,1,0:T(4,128)(2,1)S(1)}, u32[]{:S(2)}, u32[]{:S(2)}) async-start(bf16[16,4,2048]{2,1,0:T(4,128)(2,1)} %broadcast_in_dim.16), calls=%async_computation.4 | async-start | bytes 524288 | tf_op jit(solution)/shard_map/all_to_all | solution.py:41
  189.6 4.4 %copy-start.16 = (bf16[128,64]{0,1:T(8,128)(2,1)S(1)}, bf16[128,64]{0,1:T(8,128)(2,1)}, u32[]{:S(2)}) copy-start(bf16[128,64]{0,1:T(8,128)(2,1)} %param.38) | copy-start | bytes 49156
  189.6 21.2 %all-to-all-start.5 = ((bf16[32,2,2048]{2,1,0:T(2,128)(2,1)}), bf16[32,2,2048]{2,1,0:T(2,128)(2,1)S(1)}, u32[]{:S(2)}, u32[]{:S(2)}) async-start(bf16[32,2,2048]{2,1,0:T(2,128)(2,1)} %reshape.352), calls=%async_computation.5 | async-start | bytes 524288 | tf_op jit(solution)/shard_map/all_to_all | solution.py:222
  (3 other events, 2.1 us)
where the time goes:
time: 218 us; the launch traced here: 217 us
  waiting for transfers between devices  77.5 us (36%)
  starting transfers between devices  48.3 us (22%)
  blocking collectives  38.1 us (17%)
  local copies, waits for them, and re-layouts  32.7 us (15%)
  other arithmetic  17.1 us (8%)
    all_gather x2, blocking collectives, total_of_pieces(): pieces = lax.all_gather(value, axis).astype(jnp.float32)  38.1 us
    all_to_all x2, waiting for transfers between devices, summed_on_arrival(): lax.all_to_all(pieces, axis, split_axis=0, concat_axis=0, tiled=True)  27.8 us
    all_to_all x3, waiting for transfers between devices, from_everyone(): lax.all_to_all(jnp.broadcast_to(value[None], (peers, *value.shape)), axis...  27.7 us
    all_to_all x2, starting transfers between devices, summed_on_arrival(): lax.all_to_all(pieces, axis, split_axis=0, concat_axis=0, tiled=True)  18.4 us
    all_to_all x3, starting transfers between devices, from_everyone(): lax.all_to_all(jnp.broadcast_to(value[None], (peers, *value.shape)), axis...  13.7 us
    unnamed x1, other arithmetic  11.5 us
    all_to_all x1, waiting for transfers between devices, sum_at_owner(): lax.all_to_all(pieces, axis, split_axis=0, concat_axis=0, tiled=True)  11.4 us
    all_to_all x1, waiting for transfers between devices, per_device(): lax.all_to_all(outgoing, 'ep', split_axis=0, concat_axis=2, tiled=True)[0]  10.5 us
  transfers between devices with their start and end apart: 8, of which 7 were waited for; matrix products, arithmetic and copies ran while one was open for 5% of the time, Pallas kernels for 0%

commit v1 on v0

--- a/solution.py
+++ b/solution.py
@@ -1,8 +1,10 @@
+import functools
 import math
 import jax
 import jax.numpy as jnp
 from jax import lax
 from jax.sharding import PartitionSpec as P
+from jax.lax import all_to_all, axis_size
 
 D = 2048
 KEY_DIM = 128
@@ -10,6 +12,16 @@
 norm_eps = 1e-06
 clamp_limit = 7.0
 gate_alpha = 1.702
+
+
+def watch_pools(local_array, link_axis):
+    later = axis_size(link_axis)
+    view_out = jnp.stack(jnp.split(local_array, later, axis=2))
+    g_now = all_to_all(view_out, link_axis, 0, 0)
+    return jnp.concatenate(g_now, axis=0)
+
+
+launch_the_stocks = functools.partial(watch_pools, link_axis="ep")
 
 
 def split_up(value, dim, peers):
@@ -219,7 +231,7 @@
     )
     expert_part = rounded_product(hidden, expert_down[0]).astype(jnp.float32)
     expert_sum = nested_sum(expert_part.astype(jnp.bfloat16), "tp").astype(jnp.bfloat16)
-    returned = lax.all_to_all(expert_sum[None], "ep", split_axis=2, concat_axis=0, tiled=True)
+    returned = launch_the_stocks(expert_sum[None])
     picked = returned.reshape(ep_count * slot_count, local_width)[target]
     picked = picked.reshape(batch_rows, topk_count, local_width).astype(jnp.float32)
     routed = jnp.sum(picked * route_weight[:, :, None], axis=1)

time: 218 us -> 206 us (0.945)
  other arithmetic: 17.1 us -> 5.6 us
    unnamed x1 -> x0, other arithmetic: 11.5 us -> none
    unnamed x50 -> x80, local copies, waits for them, and re-layouts: 10.1 us -> 10.8 us
  transfers between devices with their start and end apart: 8 -> 8, of which waited for: 7 -> 7; matrix products, arithmetic and copies ran while one was open for 5% -> 6% of each run, Pallas kernels for 0% -> 0%
where the time goes in v1:
time: 206 us; the launch traced here: 204 us
  waiting for transfers between devices  77.5 us (38%)
  starting transfers between devices  48.3 us (23%)
  blocking collectives  38.1 us (18%)
  local copies, waits for them, and re-layouts  31.4 us (15%)
  other arithmetic  5.6 us (3%)
  matrix products  2.16 us (1%)
    all_gather x2, blocking collectives, total_of_pieces(): pieces = lax.all_gather(value, axis).astype(jnp.float32)  38.1 us
    all_to_all x2, waiting for transfers between devices, summed_on_arrival(): lax.all_to_all(pieces, axis, split_axis=0, concat_axis=0, tiled=True)  27.8 us
    all_to_all x3, waiting for transfers between devices, from_everyone(): lax.all_to_all(jnp.broadcast_to(value[None], (peers, *value.shape)), axis...  27.7 us
    all_to_all x2, starting transfers between devices, summed_on_arrival(): lax.all_to_all(pieces, axis, split_axis=0, concat_axis=0, tiled=True)  18.4 us
    all_to_all x3, starting transfers between devices, from_everyone(): lax.all_to_all(jnp.broadcast_to(value[None], (peers, *value.shape)), axis...  13.7 us
    all_to_all x1, waiting for transfers between devices, sum_at_owner(): lax.all_to_all(pieces, axis, split_axis=0, concat_axis=0, tiled=True)  11.4 us
    unnamed x80, local copies, waits for them, and re-layouts  10.8 us
    all_to_all x1, waiting for transfers between devices, per_device(): lax.all_to_all(outgoing, 'ep', split_axis=0, concat_axis=2, tiled=True)[0]  10.5 us
  transfers between devices with their start and end apart: 8, of which 7 were waited for; matrix products, arithmetic and copies ran while one was open for 6% of the time, Pallas kernels for 0%

profile of v1, /device:TPU:1, one launch (start us, length us, event | category | flops | bytes accessed | tf_op | source)
XLA Modules:
  0.0 204.5 jit_solution(17358102217650725900)
XLA Ops:
  3.7 13.8 %all-to-all-start = ((f32[32,8,769]{2,1,0:T(8,128)}), f32[32,8,769]{2,1,0:T(8,128)S(1)}, u32[]{:S(2)}, u32[]{:S(2)}) async-start(f32[32,8,769]{2,1,0:T(8,128)} %pad_maximum_fusion), calls=%async_computation | async-start | bytes 1835008 | tf_op jit(solution)/shard_map/all_to_all | solution.py:35
  18.0 1.0 fusion.97
  19.7 21.4 %all-to-all-done = f32[32,8,769]{2,1,0:T(8,128)S(1)} async-done(((f32[32,8,769]{2,1,0:T(8,128)}), f32[32,8,769]{2,1,0:T(8,128)S(1)}, u32[]{:S(2)}, u32[]{:S(2)}) %all-to-all-start) | async-done | bytes 787488 | tf_op jit(solution)/shard_map/all_to_all | solution.py:35
  43.4 6.0 %all-to-all-start.1 = ((bf16[32,8,256]{2,1,0:T(8,128)(2,1)}), bf16[32,8,256]{2,1,0:T(8,128)(2,1)S(1)}, u32[]{:S(2)}, u32[]{:S(2)}) async-start(bf16[32,8,256]{2,1,0:T(8,128)(2,1)} %broadcast_in_dim.13), calls=%async_computation.1 | async-start | bytes 262144 | tf_op jit(solution)/shard_map/all_to_all | solution.py:53
  50.3 4.3 %scatter_custom_fusion = s32[2048]{0:T(1024)S(1)} fusion(s32[1024]{0:T(1024)S(1)} %bitcast.210, s32[1024]{0:T(1024)S(1)} %add_select_fusion, s32[]{:T(128)} %constant.47.clone.1), kind=kCustom, calls=%fused_computation.181 | custom fusion | bytes 8196 | tf_op jit(solution)/shard_map/scatter | solution.py:137
  54.6 4.3 %all-to-all-done.1 = bf16[32,8,256]{2,1,0:T(8,128)(2,1)S(1)} async-done(((bf16[32,8,256]{2,1,0:T(8,128)(2,1)}), bf16[32,8,256]{2,1,0:T(8,128)(2,1)S(1)}, u32[]{:S(2)}, u32[]{:S(2)}) %all-to-all-start.1) | async-done | bytes 131104 | tf_op jit(solution)/shard_map/all_to_all | solution.py:53
  59.0 22.2 %all-gather = bf16[4096,64]{0,1:T(8,128)(2,1)S(1)} all-gather(bf16[256,64]{0,1:T(8,128)(2,1)S(1)} %convolution_convert_fusion.2), channel_id=2, replica_groups=mesh['ep'=32,'tp'=16] {'tp'}, dimensions={0}, use_global_device_ids=true | all-gather | bytes 557056 | tf_op jit(solution)/shard_map/all_gather | solution.py:70
  83.7 6.2 %gather_fusion = bf16[2048,64]{1,0:T(8,128)(2,1)S(1)} fusion(bf16[257,64]{1,0:T(8,128)(2,1)S(1)} %concatenate.47, s32[2048]{0:T(1024)S(1)} %fusion.55), kind=kCustom, calls=%fused_computation | custom fusion | bytes 532480 | tf_op jit(solution)/shard_map/gather | solution.py:215
  89.8 1.1 reshape.345
  90.9 4.1 %all-to-all-start.2 = ((bf16[32,2,2048]{2,1,0:T(2,128)(2,1)}), bf16[32,2,2048]{2,1,0:T(2,128)(2,1)S(1)}, u32[]{:S(2)}, u32[]{:S(2)}) async-start(bf16[32,2,2048]{2,1,0:T(2,128)(2,1)} %reshape.345), calls=%async_computation.2 | async-start | bytes 524288 | tf_op jit(solution)/shard_map/all_to_all | solution.py:216
  95.0 1.1 all_to_all.38
  96.1 10.5 %all-to-all-done.2 = bf16[32,2,2048]{2,1,0:T(2,128)(2,1)S(1)} async-done(((bf16[32,2,2048]{2,1,0:T(2,128)(2,1)}), bf16[32,2,2048]{2,1,0:T(2,128)(2,1)S(1)}, u32[]{:S(2)}, u32[]{:S(2)}) %all-to-all-start.2) | async-done | bytes 262176 | tf_op jit(solution)/shard_map/all_to_all | solution.py:216
  106.6 4.5 %all-to-all-start.6 = ((f32[32,1,2064]{2,1,0:T(1,128)}), f32[32,1,2064]{2,1,0:T(1,128)S(1)}, u32[]{:S(2)}, u32[]{:S(2)}) async-start(f32[32,1,2064]{2,1,0:T(1,128)} %all_to_all.38), calls=%async_computation.6 | async-start | bytes 557056 | tf_op jit(solution)/shard_map/all_to_all | solution.py:35
  115.5 6.4 %all-to-all-done.6 = f32[32,1,2064]{2,1,0:T(1,128)S(1)} async-done(((f32[32,1,2064]{2,1,0:T(1,128)}), f32[32,1,2064]{2,1,0:T(1,128)S(1)}, u32[]{:S(2)}, u32[]{:S(2)}) %all-to-all-start.6) | async-done | bytes 264224 | tf_op jit(solution)/shard_map/all_to_all | solution.py:35
  121.9 7.8 %all-to-all-start.3 = ((bf16[16,4,2048]{2,1,0:T(4,128)(2,1)}), bf16[16,4,2048]{2,1,0:T(4,128)(2,1)S(1)}, u32[]{:S(2)}, u32[]{:S(2)}) async-start(bf16[16,4,2048]{2,1,0:T(4,128)(2,1)} %reshape.297), calls=%async_computation.3 | async-start | bytes 524288 | tf_op jit(solution)/shard_map/all_to_all | solution.py:76
  129.9 11.4 %all-to-all-done.3 = bf16[16,4,2048]{2,1,0:T(4,128)(2,1)S(1)} async-done(((bf16[16,4,2048]{2,1,0:T(4,128)(2,1)}), bf16[16,4,2048]{2,1,0:T(4,128)(2,1)S(1)}, u32[]{:S(2)}, u32[]{:S(2)}) %all-to-all-start.3) | async-done | bytes 262176 | tf_op jit(solution)/shard_map/all_to_all | solution.py:76
  142.1 3.9 %all-to-all-start.7 = ((f32[32,1,2064]{2,1,0:T(1,128)}), f32[32,1,2064]{2,1,0:T(1,128)S(1)}, u32[]{:S(2)}, u32[]{:S(2)}) async-start(f32[32,1,2064]{2,1,0:T(1,128)} %broadcast_in_dim.18), calls=%async_computation.7 | async-start | bytes 557056 | tf_op jit(solution)/shard_map/all_to_all | solution.py:53
  146.1 13.0 %all-to-all-done.7 = f32[32,1,2064]{2,1,0:T(1,128)S(1)} async-done(((f32[32,1,2064]{2,1,0:T(1,128)}), f32[32,1,2064]{2,1,0:T(1,128)S(1)}, u32[]{:S(2)}, u32[]{:S(2)}) %all-to-all-start.7) | async-done | bytes 264224 | tf_op jit(solution)/shard_map/all_to_all | solution.py:53
  159.9 3.9 %all-to-all-start.4 = ((bf16[16,4,2048]{2,1,0:T(4,128)(2,1)}), bf16[16,4,2048]{2,1,0:T(4,128)(2,1)S(1)}, u32[]{:S(2)}, u32[]{:S(2)}) async-start(bf16[16,4,2048]{2,1,0:T(4,128)(2,1)} %broadcast_in_dim.16), calls=%async_computation.4 | async-start | bytes 524288 | tf_op jit(solution)/shard_map/all_to_all | solution.py:53
  165.1 10.5 %all-to-all-done.4 = bf16[16,4,2048]{2,1,0:T(4,128)(2,1)S(1)} async-done(((bf16[16,4,2048]{2,1,0:T(4,128)(2,1)}), bf16[16,4,2048]{2,1,0:T(4,128)(2,1)S(1)}, u32[]{:S(2)}, u32[]{:S(2)}) %all-to-all-start.4) | async-done | bytes 262176 | tf_op jit(solution)/shard_map/all_to_all | solution.py:53
  177.4 1.1 reshape.347
  178.5 4.4 %all-to-all-start.5 = ((bf16[32,2,2048]{2,1,0:T(2,128)(2,1)}), bf16[32,2,2048]{2,1,0:T(2,128)(2,1)S(1)}, u32[]{:S(2)}, u32[]{:S(2)}) async-start(bf16[32,2,2048]{2,1,0:T(2,128)(2,1)} %reshape.347), calls=%async_computation.5 | async-start | bytes 524288 | tf_op jit(solution)/shard_map/all_to_all | solution.py:20
  183.1 15.9 %all-gather.1 = bf16[4096,64]{0,1:T(8,128)(2,1)S(1)} all-gather(bf16[256,64]{0,1:T(8,128)(2,1)S(1)} %convolution_convert_fusion.1), channel_id=3, replica_groups=mesh['ep'=32,'tp'=16] {'tp'}, dimensions={0}, use_global_device_ids=true | all-gather | bytes 557056 | tf_op jit(solution)/shard_map/all_gather | solution.py:70
  200.0 3.2 %gather_fusion.1 = bf16[1024,64]{1,0:T(8,128)(2,1)S(1)} fusion(bf16[2048,64]{1,0:T(8,128)(2,1)S(1)} %bitcast.203, s32[1024]{0:T(1024)S(1)} %broadcast_clamp_fusion), kind=kCustom, calls=%fused_computation.1 | custom fusion | bytes 266240 | tf_op jit(solution)/shard_map/gather | solution.py:235
  (148 shorter events, 21.2 us)
Async XLA Ops:
  0.6 112.9 %copy-start = (bf16[1,128,2048]{2,1,0:T(8,128)(2,1)S(1)}, bf16[1,128,2048]{2,1,0:T(8,128)(2,1)}, u32[]{:S(2)}) copy-start(bf16[1,128,2048]{2,1,0:T(8,128)(2,1)} %param.33) | copy-start | bytes 1572868
  1.7 0.8 copy-start.5
  1.7 0.8 copy-start.6
  1.7 0.8 copy-start.8
  1.7 0.7 copy-start.9
  1.7 0.7 copy-start.15
  3.7 13.9 %copy-start.17 = (s32[8]{0:T(128)S(1)}, s32[8]{0:T(128)}, u32[]{:S(2)}) copy-start(s32[8]{0:T(128)} %param.29) | copy-start | bytes 100
  3.7 13.9 %copy-start.12 = (s32[256,4]{0,1:T(4,128)S(1)}, s32[256,4]{0,1:T(4,128)}, u32[]{:S(2)}) copy-start(s32[256,4]{0,1:T(4,128)} %param.34) | copy-start | bytes 12292
  3.7 37.4 %all-to-all-start = ((f32[32,8,769]{2,1,0:T(8,128)}), f32[32,8,769]{2,1,0:T(8,128)S(1)}, u32[]{:S(2)}, u32[]{:S(2)}) async-start(f32[32,8,769]{2,1,0:T(8,128)} %pad_maximum_fusion), calls=%async_computation | async-start | bytes 1835008 | tf_op jit(solution)/shard_map/all_to_all | solution.py:35
  17.6 24.1 %copy-start.2 = (f32[8,1,128,256]{3,2,1,0:T(8,128)S(1)}, f32[8,1,128,256]{3,2,1,0:T(8,128)}, u32[]{:S(2)}) copy-start(f32[8,1,128,256]{3,2,1,0:T(8,128)} %param.28) | copy-start | bytes 3145732
  41.9 39.3 %copy-start.1 = (f32[8,1,128,256]{3,2,1,0:T(8,128)}, f32[8,1,128,256]{3,2,1,0:T(8,128)S(1)}, u32[]{:S(2)}) copy-start(f32[8,1,128,256]{3,2,1,0:T(8,128)S(1)} %multiply_add_fusion) | copy-start | bytes 3145732
  43.4 15.4 %all-to-all-start.1 = ((bf16[32,8,256]{2,1,0:T(8,128)(2,1)}), bf16[32,8,256]{2,1,0:T(8,128)(2,1)S(1)}, u32[]{:S(2)}, u32[]{:S(2)}) async-start(bf16[32,8,256]{2,1,0:T(8,128)(2,1)} %broadcast_in_dim.13), calls=%async_computation.1 | async-start | bytes 262144 | tf_op jit(solution)/shard_map/all_to_all | solution.py:53
  49.4 9.4 %copy-start.7 = (bf16[256,64]{0,1:T(8,128)(2,1)S(1)}, bf16[256,64]{0,1:T(8,128)(2,1)}, u32[]{:S(2)}) copy-start(bf16[256,64]{0,1:T(8,128)(2,1)} %param.27) | copy-start | bytes 98308
  81.9 0.7 copy-start.11
  90.9 15.7 %all-to-all-start.2 = ((bf16[32,2,2048]{2,1,0:T(2,128)(2,1)}), bf16[32,2,2048]{2,1,0:T(2,128)(2,1)S(1)}, u32[]{:S(2)}, u32[]{:S(2)}) async-start(bf16[32,2,2048]{2,1,0:T(2,128)(2,1)} %reshape.345), calls=%async_computation.2 | async-start | bytes 524288 | tf_op jit(solution)/shard_map/all_to_all | solution.py:216
  106.6 15.3 %all-to-all-start.6 = ((f32[32,1,2064]{2,1,0:T(1,128)}), f32[32,1,2064]{2,1,0:T(1,128)S(1)}, u32[]{:S(2)}, u32[]{:S(2)}) async-start(f32[32,1,2064]{2,1,0:T(1,128)} %all_to_all.38), calls=%async_computation.6 | async-start | bytes 557056 | tf_op jit(solution)/shard_map/all_to_all | solution.py:35
  112.2 1.0 copy-start.3
  113.3 1.0 copy-start.4
  121.9 19.4 %all-to-all-start.3 = ((bf16[16,4,2048]{2,1,0:T(4,128)(2,1)}), bf16[16,4,2048]{2,1,0:T(4,128)(2,1)S(1)}, u32[]{:S(2)}, u32[]{:S(2)}) async-start(bf16[16,4,2048]{2,1,0:T(4,128)(2,1)} %reshape.297), calls=%async_computation.3 | async-start | bytes 524288 | tf_op jit(solution)/shard_map/all_to_all | solution.py:76
  142.1 17.0 %all-to-all-start.7 = ((f32[32,1,2064]{2,1,0:T(1,128)}), f32[32,1,2064]{2,1,0:T(1,128)S(1)}, u32[]{:S(2)}, u32[]{:S(2)}) async-start(f32[32,1,2064]{2,1,0:T(1,128)} %broadcast_in_dim.18), calls=%async_computation.7 | async-start | bytes 557056 | tf_op jit(solution)/shard_map/all_to_all | solution.py:53
  159.9 3.9 %copy-start.14 = (f32[256,4]{0,1:T(4,128)S(1)}, f32[256,4]{0,1:T(4,128)}, u32[]{:S(2)}) copy-start(f32[256,4]{0,1:T(4,128)} %param.35) | copy-start | bytes 12292
  159.9 15.7 %all-to-all-start.4 = ((bf16[16,4,2048]{2,1,0:T(4,128)(2,1)}), bf16[16,4,2048]{2,1,0:T(4,128)(2,1)S(1)}, u32[]{:S(2)}, u32[]{:S(2)}) async-start(bf16[16,4,2048]{2,1,0:T(4,128)(2,1)} %broadcast_in_dim.16), calls=%async_computation.4 | async-start | bytes 524288 | tf_op jit(solution)/shard_map/all_to_all | solution.py:53
  178.5 4.4 %copy-start.16 = (bf16[128,64]{0,1:T(8,128)(2,1)S(1)}, bf16[128,64]{0,1:T(8,128)(2,1)}, u32[]{:S(2)}) copy-start(bf16[128,64]{0,1:T(8,128)(2,1)} %param.38) | copy-start | bytes 49156
  178.5 21.2 %all-to-all-start.5 = ((bf16[32,2,2048]{2,1,0:T(2,128)(2,1)}), bf16[32,2,2048]{2,1,0:T(2,128)(2,1)S(1)}, u32[]{:S(2)}, u32[]{:S(2)}) async-start(bf16[32,2,2048]{2,1,0:T(2,128)(2,1)} %reshape.347), calls=%async_computation.5 | async-start | bytes 524288 | tf_op jit(solution)/shard_map/all_to_all | solution.py:20
  (3 other events, 2.1 us)
